TPU v7x, 32 devices: a whole 2x2x4 slice. The times are simulated.
32 devices in a mesh: sp: 8 (over z, x), tp: 4 (over y, core).
Axes of the slice: x: 2, y: 2, z: 4, core: 2. Of those that a mesh axis runs over, the one named last changes fastest.
Arguments:
- queries: bfloat16 [1024, 1024], P('sp', 'tp'), may hold values from -12 to 12
- keys: bfloat16 [1024, 256], P('sp', 'tp'), may hold values from -12 to 12
- values: bfloat16 [1024, 256], P('sp', 'tp'), may hold values from -6 to 6
- log_gate: float32 [16, 1024], P('tp', 'sp'), may hold values from -0.2 to 0, as said below
- log_sum: float32 [16, 1024], P('tp', 'sp'), may hold values from -100 to 100, as said below
- output: bfloat16 [1024, 1024], P('sp', 'tp'), may hold values from -6 to 6
- cotangent: bfloat16 [1024, 1024], P('sp', 'tp'), may hold values from -12 to 12
- normed: bfloat16 [1024, 2048], P('sp', 'tp'), may hold values from -8 to 8
Outputs:
- query_grad: bfloat16 [1024, 1024], P('sp', 'tp')
- key_grad: bfloat16 [1024, 256], P('sp', 'tp')
- value_grad: bfloat16 [1024, 256], P('sp', 'tp')
- weight_grad: float32 [2048, 256], P('sp', 'tp')
Inputs may be any that keep to these rules, and one draw needn't show every extreme that they name: `log_gate`: every entry is negative. log_sum[h, t] is the logarithm of the sum over s <= t of exp of the scores of the steps (before log_sum is subtracted), computed from the given queries, keys and log_gate.
All inputs are finite; a program needn't handle non-finite values.
Results may differ from a plain program's by a relative error of at most 0.005.
Values may be sent and summed in bfloat16 or wider, within the bound.
A program may use at most 64 MiB of HBM per device.

v0:
```python
import jax
import jax.numpy as jnp
from jax import lax
from jax.sharding import PartitionSpec as P

HDIM = 64


NEG_LARGE = -1e30


def prefix(x, axis, combine, identity):
    size, place = (lax.axis_size(axis), lax.axis_index(axis))
    everything = lax.all_gather(x, axis)
    start = jnp.broadcast_to(jnp.asarray(identity, x.dtype), x.shape)

    def hop(k, before):
        reached = k < place
        new = combine(before, everything[k])
        return jnp.where(reached, new, before)

    return lax.fori_loop(0, size, hop, start)


def shifted(x, axis, by):
    size = lax.axis_size(axis)
    pairs = [(i, i + by) for i in range(size) if 0 <= i + by < size]
    return lax.ppermute(x, axis, pairs)


def shifted_2(x, axis, by):
    size = lax.axis_size(axis)
    return lax.ppermute(x, axis, [(i, (i + by) % size) for i in range(size)])


def add_pair(earlier, later):
    return earlier + later


def body(queries, keys, values, log_gate, log_sum, output, cotangent, normed):
    tokens = queries.shape[0]
    head_count = log_gate.shape[0]
    kv_width = keys.shape[1]
    kv_heads = kv_width // HDIM
    groups = head_count // kv_heads
    inverse_root = HDIM ** (-0.5)
    devices = lax.axis_size("sp")
    my_index = lax.axis_index("sp")
    depth = 8
    totals = jnp.sum(log_gate, axis=1)
    before = prefix(totals, "sp", add_pair, jnp.zeros_like(totals))
    cumulative = jnp.cumsum(log_gate, axis=1) + before[:, None]
    row_terms = jnp.sum(
        (output.astype(jnp.float32) * cotangent.astype(jnp.float32)).reshape(
            tokens, head_count, HDIM
        ),
        axis=2,
    ).T
    query_split = queries.reshape(tokens, kv_heads, groups, HDIM)
    cotan_split = cotangent.reshape(tokens, kv_heads, groups, HDIM)
    cum_rows = cumulative.reshape(kv_heads, groups, tokens)
    lse_rows = log_sum.reshape(kv_heads, groups, tokens)
    term_rows = row_terms.reshape(kv_heads, groups, tokens)
    positions = my_index * tokens + jnp.arange(tokens)
    last_row = my_index * tokens + tokens - 1

    def visit_bundle(bundle, bundle_cum, key_pos):
        count = bundle.shape[0]
        block_rows = bundle.shape[1]
        key_rows = count * block_rows
        flat = bundle.reshape(key_rows, 2 * kv_width)
        flat_cum = jnp.transpose(bundle_cum, (1, 0, 2)).reshape(kv_heads, groups, key_rows)
        flat_pos = key_pos.reshape(key_rows)
        key_part = flat[:, :kv_width].reshape(key_rows, kv_heads, HDIM)
        value_part = flat[:, kv_width:].reshape(key_rows, kv_heads, HDIM)

        def attend(unused):
            scores = (
                jnp.einsum(
                    "qhgd,khd->hgqk", query_split, key_part, preferred_element_type=jnp.float32
                )
                * inverse_root
            )
            scores = (
                scores + cum_rows[:, :, :, None] - flat_cum[:, :, None, :] - lse_rows[:, :, :, None]
            )
            allowed = flat_pos[None, :] <= positions[:, None]
            weights = jnp.exp(jnp.where(allowed, scores, NEG_LARGE))
            upstream = jnp.einsum(
                "qhgd,khd->hgqk", cotan_split, value_part, preferred_element_type=jnp.float32
            )
            dscore_low = (weights * (upstream - term_rows[:, :, :, None])).astype(jnp.bfloat16)
            weights_low = weights.astype(jnp.bfloat16)
            query_add = (
                jnp.einsum(
                    "hgqk,khd->qhgd", dscore_low, key_part, preferred_element_type=jnp.float32
                )
                * inverse_root
            )
            key_add = (
                jnp.einsum(
                    "hgqk,qhgd->khd", dscore_low, query_split, preferred_element_type=jnp.float32
                )
                * inverse_root
            )
            value_add = jnp.einsum(
                "hgqk,qhgd->khd", weights_low, cotan_split, preferred_element_type=jnp.float32
            )
            joined = jnp.concatenate(
                [key_add.reshape(key_rows, kv_width), value_add.reshape(key_rows, kv_width)], axis=1
            )
            return (query_add, joined.reshape(count, block_rows, 2 * kv_width))

        def nothing(unused):
            return (
                jnp.zeros((tokens, kv_heads, groups, HDIM), jnp.float32),
                jnp.zeros((count, block_rows, 2 * kv_width), jnp.float32),
            )

        return lax.cond(jnp.min(flat_pos) <= last_row, attend, nothing, 0)

    stacked = jnp.concatenate([keys, values], axis=1)
    query_start = jnp.zeros((tokens, kv_heads, groups, HDIM), jnp.float32)
    copies = jnp.arange(depth)
    turns = devices // depth
    bundle_pieces = [stacked]
    bundle_cums = [cumulative]
    for step in range(1, depth):
        bundle_pieces.append(shifted(stacked, "sp", step))
        bundle_cums.append(shifted(cumulative, "sp", step))

    def turn(turn_index, state_now):
        query_total, bundle, bundle_cum, bundle_grads = state_now
        anchor = (my_index - depth * turn_index) % devices
        blocks = (anchor - copies) % devices
        key_pos = blocks[:, None] * tokens + jnp.arange(tokens)[None, :]
        query_add, grad_add = visit_bundle(bundle, bundle_cum, key_pos)
        bundle = shifted(bundle, "sp", depth)
        bundle_cum, bundle_grads = shifted_2((bundle_cum, bundle_grads + grad_add), "sp", depth)
        return (query_total + query_add, bundle, bundle_cum, bundle_grads)

    start_state = (
        query_start,
        jnp.stack(bundle_pieces),
        jnp.stack(bundle_cums),
        jnp.zeros((depth, tokens, 2 * kv_width), jnp.float32),
    )
    finished = lax.fori_loop(0, turns, turn, start_state)
    query_total = finished[0]
    final_grads = finished[3]
    gradients = final_grads[0]
    for step in range(1, depth):
        gradients = gradients + shifted(final_grads[step], "sp", -step)
    query_grad = query_total.reshape(tokens, head_count * HDIM).astype(jnp.bfloat16)
    key_grad = gradients[:, :kv_width].astype(jnp.bfloat16)
    value_grad = gradients[:, kv_width:].astype(jnp.bfloat16)
    whole_rows = lax.all_gather(normed, "tp", axis=1, tiled=True)
    weight_grad = lax.psum_scatter(
        lax.dot_general(
            whole_rows, key_grad, (((0,), (0,)), ((), ())), preferred_element_type=jnp.float32
        ),
        "sp",
        scatter_dimension=0,
        tiled=True,
    )
    return (query_grad, key_grad, value_grad, weight_grad)


def solution(mesh):
    in_specs = (
        P("sp", "tp"),
        P("sp", "tp"),
        P("sp", "tp"),
        P("tp", "sp"),
        P("tp", "sp"),
        P("sp", "tp"),
        P("sp", "tp"),
        P("sp", "tp"),
    )
    out_specs = (P("sp", "tp"), P("sp", "tp"), P("sp", "tp"), P("sp", "tp"))
    return jax.shard_map(body, mesh=mesh, in_specs=in_specs, out_specs=out_specs, check_vma=False)
```

profile of v0, /device:TPU:0, one launch (start us, length us, event | category | flops | bytes accessed | tf_op | source)
XLA Modules:
  0.0 176.8 jit_solution(9886937687388479770)
XLA Ops:
  7.2 0.8 reduce_sum.18
  8.0 1.0 reduce_window_sum.13
  9.0 1.2 dynamic-slice
  11.2 23.1 %all-reduce = f32[32]{0:T(128)S(1)} all-reduce(f32[32]{0:T(128)S(1)} %dynamic-update-slice), channel_id=2, replica_groups=mesh['sp'=8,'tp'=4] {'sp'}, use_global_device_ids=true, to_apply=%add | all-reduce | flops 32 | bytes 256
  34.7 1.6 collective-permute-start.13
  36.4 1.3 collective-permute-start.12
  37.7 1.3 collective-permute-start.11
  39.0 1.3 collective-permute-start.10
  40.3 2.5 %collective-permute-start.7 = (f32[4,128]{1,0:T(4,128)S(1)}, f32[4,128]{1,0:T(4,128)S(1)}, u32[]{:S(2)}, u32[]{:S(2)}) collective-permute-start(f32[4,128]{1,0:T(4,128)S(1)} %broadcast_add_fusion.1), channel_id=1, source_target_pairs={{0,4},{4,8},{8,12},{12,16},{16,20},{20,24},{24,28},{1,5},{5,9},{9,... | collective-permute-start | bytes 6152 | tf_op jit(solution)/shard_map/ppermute | solution.py:28
  42.8 0.7 iota_add_fusion
  43.5 0.8 copy.33
  44.3 0.8 copy.34
  45.2 1.0 copy.35
  46.2 1.0 copy.36
  47.9 2.5 %collective-permute-start.8 = (f32[4,128]{1,0:T(4,128)S(1)}, f32[4,128]{1,0:T(4,128)S(1)}, u32[]{:S(2)}, u32[]{:S(2)}) collective-permute-start(f32[4,128]{1,0:T(4,128)S(1)} %broadcast_add_fusion.1), channel_id=1, source_target_pairs={{0,8},{4,12},{8,16},{12,20},{16,24},{20,28},{1,9},{5,13},{9,17},{1... | collective-permute-start | bytes 6152 | tf_op jit(solution)/shard_map/ppermute | solution.py:28
  50.4 1.3 collective-permute-done.8
  51.7 3.9 %collective-permute-start.9 = (f32[4,128]{1,0:T(4,128)S(1)}, f32[4,128]{1,0:T(4,128)S(1)}, u32[]{:S(2)}, u32[]{:S(2)}) collective-permute-start(f32[4,128]{1,0:T(4,128)S(1)} %broadcast_add_fusion.1), channel_id=1, source_target_pairs={{0,12},{4,16},{8,20},{12,24},{16,28},{1,13},{5,17},{9,21},{13,25},... | collective-permute-start | bytes 6152 | tf_op jit(solution)/shard_map/ppermute | solution.py:28
  55.6 1.3 collective-permute-done.9
  56.9 5.1 %collective-permute-start.5 = (bf16[128,128]{1,0:T(8,128)(2,1)S(1)}, bf16[128,128]{1,0:T(8,128)(2,1)S(1)}, u32[]{:S(2)}, u32[]{:S(2)}) collective-permute-start(bf16[128,128]{1,0:T(8,128)(2,1)S(1)} %get-tuple-element.251), channel_id=1, source_target_pairs={{0,24},{4,28},{1,25},{5,29},{2,26},{6,30},{3,27},{7,31}} | collective-permute-start | bytes 98312 | tf_op jit(solution)/shard_map/ppermute | solution.py:28
  62.0 1.3 collective-permute-start.4
  63.3 1.3 collective-permute-start.3
  64.6 1.6 collective-permute-start.2
  66.3 3.0 %collective-permute-start = (bf16[128,128]{1,0:T(8,128)(2,1)S(1)}, bf16[128,128]{1,0:T(8,128)(2,1)S(1)}, u32[]{:S(2)}, u32[]{:S(2)}) collective-permute-start(bf16[128,128]{1,0:T(8,128)(2,1)S(1)} %get-tuple-element.251), channel_id=1, source_target_pairs={{0,4},{4,8},{8,12},{12,16},{16,20},{20,24},{24,28},{1,5},{5,9},{9,... | collective-permute-start | bytes 98312 | tf_op jit(solution)/shard_map/ppermute | solution.py:28
  69.3 1.6 collective-permute-done
  70.9 4.2 %collective-permute-start.1 = (bf16[128,128]{1,0:T(8,128)(2,1)S(1)}, bf16[128,128]{1,0:T(8,128)(2,1)S(1)}, u32[]{:S(2)}, u32[]{:S(2)}) collective-permute-start(bf16[128,128]{1,0:T(8,128)(2,1)S(1)} %get-tuple-element.251), channel_id=1, source_target_pairs={{0,8},{4,12},{8,16},{12,20},{16,24},{20,28},{1,9},{5,13},{9,17},{1... | collective-permute-start | bytes 98312 | tf_op jit(solution)/shard_map/ppermute | solution.py:28
  75.1 1.6 collective-permute-done.1
  76.7 1.6 collective-permute-start.6
  78.4 1.5 collective-permute-done.6
  79.9 5.7 %conditional.1 = (f32[8,128,128]{1,2,0:T(8,128)S(1)}, bf16[128,256]{1,0:T(8,128)(2,1)S(1)}) conditional(s32[]{:T(128)} %convert_element_type.39, () %tuple.37, (s32[8,128]{1,0:T(8,128)S(1)}, s32[]{:T(128)}, s32[128]{0:T(128)S(1)}, bf16[8,128,128]{2,1,0:T(8,128)(2,1)S(1)}, bf16[128,256]{1,0:T(8,128)(2,1)}, /*index=5*/f32[4,128]{1,0:T(4,128)S(1)}, ...), branch_computations={%region_6.7_spmd, %region_7.8_spmd} | conditional | flops 340656256 | bytes 13856276 | solution.py:120
  79.9 1.0 copy.40
  80.9 1.0 copy.38
  82.1 1.5 fusion.21
  83.6 0.4 convolution_bitcast_fusion
  84.0 0.5 fusion.6
  84.5 0.3 fusion.9
  84.8 0.4 fusion.8
  85.7 1.3 collective-permute-start.15
  87.0 1.3 collective-permute-start.21
  88.3 1.3 collective-permute-start.20
  89.6 1.3 collective-permute-start.19
  90.9 1.3 collective-permute-start.18
  92.2 1.3 collective-permute-start.17
  93.5 2.3 %collective-permute-done.21 = f32[128,128]{0,1:T(8,128)S(1)} collective-permute-done((f32[128,128]{0,1:T(8,128)S(1)}, f32[128,128]{0,1:T(8,128)S(1)}, u32[]{:S(2)}, u32[]{:S(2)}) %collective-permute-start.21) | collective-permute-done | bytes 65568 | tf_op jit(solution)/shard_map/ppermute | solution.py:28
  95.8 1.3 collective-permute-start.16
  97.1 7.2 %all_gather.11 = bf16[128,2048]{1,0:T(8,128)(2,1)S(1)} all-gather(bf16[128,512]{1,0:T(8,128)(2,1)S(1)} %copy-done), channel_id=1, replica_groups=mesh['sp'=8,'tp'=4] {'tp'}, dimensions={1}, use_global_device_ids=true | all-gather | bytes 655360 | tf_op jit(solution)/shard_map/all_gather | solution.py:157
  104.4 0.6 fusion.22
  105.0 1.0 convolution_bitcast_fusion.2
  106.1 63.9 %reduce-scatter.2.cloned.1.call-done = f32[256,64]{0,1:T(8,128)} async-done(((f32[2048,64]{0,1:T(8,128)}), f32[256,64]{0,1:T(8,128)}) %reduce-scatter.2.cloned.1.call-update) | async-done | bytes 65552 | tf_op jit(solution)/shard_map/reduce_scatter | solution.py:158
  (66 shorter events, 1.8 us)
Async XLA Ops:
  7.2 162.8 %reduce-scatter.2.cloned.1.call-start = ((), (), s32[]{:S(2)}) async-start(), calls=%async_computation.1 | async-start | bytes 589824 | tf_op jit(solution)/shard_map/reduce_scatter | solution.py:158
  34.7 31.6 %collective-permute-start.13 = (f32[4,128]{1,0:T(4,128)S(1)}, f32[4,128]{1,0:T(4,128)S(1)}, u32[]{:S(2)}, u32[]{:S(2)}) collective-permute-start(f32[4,128]{1,0:T(4,128)S(1)} %broadcast_add_fusion.1), channel_id=1, source_target_pairs={{0,28},{1,29},{2,30},{3,31}} | collective-permute-start | bytes 6152 | tf_op jit(solution)/shard_map/ppermute | solution.py:28
  36.4 28.2 %collective-permute-start.12 = (f32[4,128]{1,0:T(4,128)S(1)}, f32[4,128]{1,0:T(4,128)S(1)}, u32[]{:S(2)}, u32[]{:S(2)}) collective-permute-start(f32[4,128]{1,0:T(4,128)S(1)} %broadcast_add_fusion.1), channel_id=1, source_target_pairs={{0,24},{4,28},{1,25},{5,29},{2,26},{6,30},{3,27},{7,31}} | collective-permute-start | bytes 6152 | tf_op jit(solution)/shard_map/ppermute | solution.py:28
  37.7 25.6 %collective-permute-start.11 = (f32[4,128]{1,0:T(4,128)S(1)}, f32[4,128]{1,0:T(4,128)S(1)}, u32[]{:S(2)}, u32[]{:S(2)}) collective-permute-start(f32[4,128]{1,0:T(4,128)S(1)} %broadcast_add_fusion.1), channel_id=1, source_target_pairs={{0,20},{4,24},{8,28},{1,21},{5,25},{9,29},{2,22},{6,26},{10,30},{3... | collective-permute-start | bytes 6152 | tf_op jit(solution)/shard_map/ppermute | solution.py:28
  39.0 23.0 %collective-permute-start.10 = (f32[4,128]{1,0:T(4,128)S(1)}, f32[4,128]{1,0:T(4,128)S(1)}, u32[]{:S(2)}, u32[]{:S(2)}) collective-permute-start(f32[4,128]{1,0:T(4,128)S(1)} %broadcast_add_fusion.1), channel_id=1, source_target_pairs={{0,16},{4,20},{8,24},{12,28},{1,17},{5,21},{9,25},{13,29},{2,18},{... | collective-permute-start | bytes 6152 | tf_op jit(solution)/shard_map/ppermute | solution.py:28
  40.3 7.6 %collective-permute-start.7 = (f32[4,128]{1,0:T(4,128)S(1)}, f32[4,128]{1,0:T(4,128)S(1)}, u32[]{:S(2)}, u32[]{:S(2)}) collective-permute-start(f32[4,128]{1,0:T(4,128)S(1)} %broadcast_add_fusion.1), channel_id=1, source_target_pairs={{0,4},{4,8},{8,12},{12,16},{16,20},{20,24},{24,28},{1,5},{5,9},{9,... | collective-permute-start | bytes 6152 | tf_op jit(solution)/shard_map/ppermute | solution.py:28
  47.9 3.8 %collective-permute-start.8 = (f32[4,128]{1,0:T(4,128)S(1)}, f32[4,128]{1,0:T(4,128)S(1)}, u32[]{:S(2)}, u32[]{:S(2)}) collective-permute-start(f32[4,128]{1,0:T(4,128)S(1)} %broadcast_add_fusion.1), channel_id=1, source_target_pairs={{0,8},{4,12},{8,16},{12,20},{16,24},{20,28},{1,9},{5,13},{9,17},{1... | collective-permute-start | bytes 6152 | tf_op jit(solution)/shard_map/ppermute | solution.py:28
  51.7 5.2 %collective-permute-start.9 = (f32[4,128]{1,0:T(4,128)S(1)}, f32[4,128]{1,0:T(4,128)S(1)}, u32[]{:S(2)}, u32[]{:S(2)}) collective-permute-start(f32[4,128]{1,0:T(4,128)S(1)} %broadcast_add_fusion.1), channel_id=1, source_target_pairs={{0,12},{4,16},{8,20},{12,24},{16,28},{1,13},{5,17},{9,21},{13,25},... | collective-permute-start | bytes 6152 | tf_op jit(solution)/shard_map/ppermute | solution.py:28
  56.9 21.5 %collective-permute-start.5 = (bf16[128,128]{1,0:T(8,128)(2,1)S(1)}, bf16[128,128]{1,0:T(8,128)(2,1)S(1)}, u32[]{:S(2)}, u32[]{:S(2)}) collective-permute-start(bf16[128,128]{1,0:T(8,128)(2,1)S(1)} %get-tuple-element.251), channel_id=1, source_target_pairs={{0,24},{4,28},{1,25},{5,29},{2,26},{6,30},{3,27},{7,31}} | collective-permute-start | bytes 98312 | tf_op jit(solution)/shard_map/ppermute | solution.py:28
  62.0 16.4 %collective-permute-start.4 = (bf16[128,128]{1,0:T(8,128)(2,1)S(1)}, bf16[128,128]{1,0:T(8,128)(2,1)S(1)}, u32[]{:S(2)}, u32[]{:S(2)}) collective-permute-start(bf16[128,128]{1,0:T(8,128)(2,1)S(1)} %get-tuple-element.251), channel_id=1, source_target_pairs={{0,20},{4,24},{8,28},{1,21},{5,25},{9,29},{2,22},{6,26},{10,30},{3... | collective-permute-start | bytes 98312 | tf_op jit(solution)/shard_map/ppermute | solution.py:28
  63.3 15.0 %collective-permute-start.3 = (bf16[128,128]{1,0:T(8,128)(2,1)S(1)}, bf16[128,128]{1,0:T(8,128)(2,1)S(1)}, u32[]{:S(2)}, u32[]{:S(2)}) collective-permute-start(bf16[128,128]{1,0:T(8,128)(2,1)S(1)} %get-tuple-element.251), channel_id=1, source_target_pairs={{0,16},{4,20},{8,24},{12,28},{1,17},{5,21},{9,25},{13,29},{2,18},{... | collective-permute-start | bytes 98312 | tf_op jit(solution)/shard_map/ppermute | solution.py:28
  64.6 13.7 %collective-permute-start.2 = (bf16[128,128]{1,0:T(8,128)(2,1)S(1)}, bf16[128,128]{1,0:T(8,128)(2,1)S(1)}, u32[]{:S(2)}, u32[]{:S(2)}) collective-permute-start(bf16[128,128]{1,0:T(8,128)(2,1)S(1)} %get-tuple-element.251), channel_id=1, source_target_pairs={{0,12},{4,16},{8,20},{12,24},{16,28},{1,13},{5,17},{9,21},{13,25},... | collective-permute-start | bytes 98312 | tf_op jit(solution)/shard_map/ppermute | solution.py:28
  66.3 4.6 %collective-permute-start = (bf16[128,128]{1,0:T(8,128)(2,1)S(1)}, bf16[128,128]{1,0:T(8,128)(2,1)S(1)}, u32[]{:S(2)}, u32[]{:S(2)}) collective-permute-start(bf16[128,128]{1,0:T(8,128)(2,1)S(1)} %get-tuple-element.251), channel_id=1, source_target_pairs={{0,4},{4,8},{8,12},{12,16},{16,20},{20,24},{24,28},{1,5},{5,9},{9,... | collective-permute-start | bytes 98312 | tf_op jit(solution)/shard_map/ppermute | solution.py:28
  70.9 5.8 %collective-permute-start.1 = (bf16[128,128]{1,0:T(8,128)(2,1)S(1)}, bf16[128,128]{1,0:T(8,128)(2,1)S(1)}, u32[]{:S(2)}, u32[]{:S(2)}) collective-permute-start(bf16[128,128]{1,0:T(8,128)(2,1)S(1)} %get-tuple-element.251), channel_id=1, source_target_pairs={{0,8},{4,12},{8,16},{12,20},{16,24},{20,28},{1,9},{5,13},{9,17},{1... | collective-permute-start | bytes 98312 | tf_op jit(solution)/shard_map/ppermute | solution.py:28
  76.7 3.2 %collective-permute-start.6 = (bf16[128,128]{1,0:T(8,128)(2,1)S(1)}, bf16[128,128]{1,0:T(8,128)(2,1)S(1)}, u32[]{:S(2)}, u32[]{:S(2)}) collective-permute-start(bf16[128,128]{1,0:T(8,128)(2,1)S(1)} %get-tuple-element.251), channel_id=1, source_target_pairs={{0,28},{1,29},{2,30},{3,31}} | collective-permute-start | bytes 98312 | tf_op jit(solution)/shard_map/ppermute | solution.py:28
  79.9 17.2 %copy-start = (bf16[128,512]{1,0:T(8,128)(2,1)S(1)}, bf16[128,512]{1,0:T(8,128)(2,1)}, u32[]{:S(2)}) copy-start(bf16[128,512]{1,0:T(8,128)(2,1)} %param.19) | copy-start | bytes 393220
  85.5 84.4 %copy-start.2 = (bf16[128,256]{1,0:T(8,128)(2,1)}, bf16[128,256]{1,0:T(8,128)(2,1)S(1)}, u32[]{:S(2)}) copy-start(bf16[128,256]{1,0:T(8,128)(2,1)S(1)} %get-tuple-element.241) | copy-start | bytes 196612
  85.7 6.5 %collective-permute-start.15 = (f32[128,128]{0,1:T(8,128)S(1)}, f32[128,128]{0,1:T(8,128)S(1)}, u32[]{:S(2)}, u32[]{:S(2)}) collective-permute-start(f32[128,128]{0,1:T(8,128)S(1)} %get-tuple-element.254), channel_id=1, source_target_pairs={{4,0},{8,4},{12,8},{16,12},{20,16},{24,20},{28,24},{5,1},{9,5},{13... | collective-permute-start | bytes 196616 | tf_op jit(solution)/shard_map/ppermute | solution.py:28
  87.0 8.9 %collective-permute-start.21 = (f32[128,128]{0,1:T(8,128)S(1)}, f32[128,128]{0,1:T(8,128)S(1)}, u32[]{:S(2)}, u32[]{:S(2)}) collective-permute-start(f32[128,128]{0,1:T(8,128)S(1)} %get-tuple-element.255), channel_id=1, source_target_pairs={{28,0},{29,1},{30,2},{31,3}} | collective-permute-start | bytes 196616 | tf_op jit(solution)/shard_map/ppermute | solution.py:28
  88.3 16.1 %collective-permute-start.20 = (f32[128,128]{0,1:T(8,128)S(1)}, f32[128,128]{0,1:T(8,128)S(1)}, u32[]{:S(2)}, u32[]{:S(2)}) collective-permute-start(f32[128,128]{0,1:T(8,128)S(1)} %get-tuple-element.256), channel_id=1, source_target_pairs={{24,0},{28,4},{25,1},{29,5},{26,2},{30,6},{27,3},{31,7}} | collective-permute-start | bytes 196616 | tf_op jit(solution)/shard_map/ppermute | solution.py:28
  89.6 14.8 %collective-permute-start.19 = (f32[128,128]{0,1:T(8,128)S(1)}, f32[128,128]{0,1:T(8,128)S(1)}, u32[]{:S(2)}, u32[]{:S(2)}) collective-permute-start(f32[128,128]{0,1:T(8,128)S(1)} %get-tuple-element.257), channel_id=1, source_target_pairs={{20,0},{24,4},{28,8},{21,1},{25,5},{29,9},{22,2},{26,6},{30,10},{2... | collective-permute-start | bytes 196616 | tf_op jit(solution)/shard_map/ppermute | solution.py:28
  90.9 13.5 %collective-permute-start.18 = (f32[128,128]{0,1:T(8,128)S(1)}, f32[128,128]{0,1:T(8,128)S(1)}, u32[]{:S(2)}, u32[]{:S(2)}) collective-permute-start(f32[128,128]{0,1:T(8,128)S(1)} %get-tuple-element.258), channel_id=1, source_target_pairs={{16,0},{20,4},{24,8},{28,12},{17,1},{21,5},{25,9},{29,13},{18,2},{... | collective-permute-start | bytes 196616 | tf_op jit(solution)/shard_map/ppermute | solution.py:28
  92.2 12.2 %collective-permute-start.17 = (f32[128,128]{0,1:T(8,128)S(1)}, f32[128,128]{0,1:T(8,128)S(1)}, u32[]{:S(2)}, u32[]{:S(2)}) collective-permute-start(f32[128,128]{0,1:T(8,128)S(1)} %get-tuple-element.259), channel_id=1, source_target_pairs={{12,0},{16,4},{20,8},{24,12},{28,16},{13,1},{17,5},{21,9},{25,13},... | collective-permute-start | bytes 196616 | tf_op jit(solution)/shard_map/ppermute | solution.py:28
  95.8 8.5 %collective-permute-start.16 = (f32[128,128]{0,1:T(8,128)S(1)}, f32[128,128]{0,1:T(8,128)S(1)}, u32[]{:S(2)}, u32[]{:S(2)}) collective-permute-start(f32[128,128]{0,1:T(8,128)S(1)} %get-tuple-element.260), channel_id=1, source_target_pairs={{8,0},{12,4},{16,8},{20,12},{24,16},{28,20},{9,1},{13,5},{17,9},{2... | collective-permute-start | bytes 196616 | tf_op jit(solution)/shard_map/ppermute | solution.py:28
  105.0 65.0 %copy-start.1 = (bf16[128,64]{0,1:T(8,128)(2,1)}, bf16[128,64]{0,1:T(8,128)(2,1)S(1)}, u32[]{:S(2)}) copy-start(bf16[128,64]{0,1:T(8,128)(2,1)S(1)} %get-tuple-element.262) | copy-start | bytes 49156
  (1 other events, 0.0 us)
Sparse Core Ops, SparseCore 0:
  106.2 63.7 reduce-scatter.1
where the time goes:
time: 178 us; the launch traced here: 177 us
  waiting for transfers between devices  73.4 us (41%)
  starting transfers between devices  41.6 us (23%)
  blocking collectives  30.3 us (17%)
  between operations  15.8 us (9%)
  local copies, waits for them, and re-layouts  8.07 us (5%)
  matrix products  4.19 us (2%)
  other arithmetic  3.18 us (2%)
    reduce_scatter x1, waiting for transfers between devices, body(): lax.psum_scatter(lax.dot_general(whole_rows, key_grad, (((0,), (0,)), (()...  63.9 us
    ppermute x21, starting transfers between devices, shifted(): return lax.ppermute(x, axis, pairs)  41.5 us
    unnamed x1, blocking collectives  23.1 us
    ppermute x21, waiting for transfers between devices, shifted(): return lax.ppermute(x, axis, pairs)  9.53 us
    all_gather x1, blocking collectives, body(): whole_rows = lax.all_gather(normed, 'tp', axis=1, tiled=True)  7.21 us
    unnamed x25, local copies, waits for them, and re-layouts  5.18 us
  transfers between devices with their start and end apart: 23, of which 7 were waited for; matrix products, arithmetic and copies ran while one was open for 3% of the time, Pallas kernels for 0%

commit v1 on v0

--- a/solution.py
+++ b/solution.py
@@ -1,6 +1,10 @@
+import functools
+
 import jax
 import jax.numpy as jnp
 from jax import lax
+from jax.experimental import pallas as pl
+from jax.experimental.pallas import tpu as pltpu
 from jax.sharding import PartitionSpec as P
 
 HDIM = 64
@@ -166,7 +170,258 @@
     return (query_grad, key_grad, value_grad, weight_grad)
 
 
+F32, BF16 = (jnp.float32, jnp.bfloat16)
+HBM = pl.BlockSpec(memory_space=pl.ANY)
+NT = (((1,), (1,)), ((), ()))
+NN = (((1,), (0,)), ((), ()))
+
+
+def dot(a, b, dims=NN, precision=None):
+    return lax.dot_general(a, b, dims, precision=precision, preferred_element_type=F32)
+
+
+def fused(
+    n, m,
+    q_hbm, k_hbm, v_hbm, gate_hbm, lse_hbm, out_hbm, cot_hbm, normed_hbm,
+    qg_ref, kg_ref, vg_ref, wg_ref,
+    q_in, k_in, v_in, gate_in, lse_in, out_in, cot_in,
+    normed_all, kv, gates, diag, dq, grad_send, grad_recv, grad_own, w_send, w_recv, w_own,
+    in_sem, norm_in_sem, norm_send, norm_recv, kv_send, kv_recv, gate_send, gate_recv,
+    gr_send, gr_recv, wt_send, wt_recv,
+):
+    me = lax.axis_index("sp")
+    tp = lax.axis_index("tp")
+    tokens, width = q_in.shape
+    groups = gate_in.shape[0]
+    span = groups * tokens
+    chunk = normed_all.shape[2]
+    per = normed_all.shape[0] // m
+    scale = HDIM ** (-0.5)
+
+    barrier = pltpu.get_barrier_semaphore()
+    for k in range(1, n):
+        pl.semaphore_signal(barrier, inc=1, device_id={"sp": lax.rem(me + k, n)}, device_id_type=pl.DeviceIdType.MESH)
+    for k in range(1, m):
+        pl.semaphore_signal(barrier, inc=1, device_id={"tp": lax.rem(tp + k, m)}, device_id_type=pl.DeviceIdType.MESH)
+
+    pairs = [
+        (k_hbm, k_in), (v_hbm, v_in), (gate_hbm, gate_in), (q_hbm, q_in), (cot_hbm, cot_in),
+        (out_hbm, out_in), (lse_hbm, lse_in),
+    ]
+    loads = [pltpu.make_async_copy(a, b, in_sem.at[i]) for i, (a, b) in enumerate(pairs)]
+    for load in loads:
+        load.start()
+    norm_loads = [
+        pltpu.make_async_copy(
+            normed_hbm.at[:, pl.ds(c * chunk, chunk)], normed_all.at[tp * per + c], norm_in_sem.at[c]
+        )
+        for c in range(per)
+    ]
+    for load in norm_loads:
+        load.start()
+
+    for load in loads[:3]:
+        load.wait()
+    kv[0] = jnp.concatenate([k_in[...], v_in[...]], axis=1)
+    rows = lax.broadcasted_iota(jnp.int32, (tokens, tokens), 0)
+    cols = lax.broadcasted_iota(jnp.int32, (tokens, tokens), 1)
+    gate = gate_in[...]
+    local = dot(gate, (rows <= cols).astype(F32), NN, lax.Precision.HIGHEST)
+    total = jnp.broadcast_to(jnp.sum(gate, axis=1, keepdims=True), gate.shape)
+    gates[0, 0:groups, :] = total - local
+    gates[0, groups:, :] = total
+
+    for load in norm_loads:
+        load.wait()
+    pl.semaphore_wait(barrier, n - 1 + m - 1)
+
+    def kv_copy(k):
+        where = {"sp": lax.rem(me + k, n)}
+        return (
+            pltpu.make_async_remote_copy(gates.at[0], gates.at[k], gate_send.at[k], gate_recv.at[k], where, pl.DeviceIdType.MESH),
+            pltpu.make_async_remote_copy(kv.at[0], kv.at[k], kv_send.at[k], kv_recv.at[k], where, pl.DeviceIdType.MESH),
+        )
+
+    def norm_copy(k):
+        mine = normed_all.at[pl.ds(tp * per, per)]
+        return pltpu.make_async_remote_copy(
+            mine, mine, norm_send.at[k], norm_recv.at[k], {"tp": lax.rem(tp + k, m)}, pl.DeviceIdType.MESH
+        )
+
+    def norm_arrival(k):
+        theirs = normed_all.at[pl.ds(lax.rem(tp + m - k, m) * per, per)]
+        return pltpu.make_async_remote_copy(
+            theirs, theirs, norm_send.at[k], norm_recv.at[k], {"tp": lax.rem(tp + k, m)}, pl.DeviceIdType.MESH
+        )
+
+    def grad_copy(k):
+        where = {"sp": lax.rem(me + n - k, n)}
+        return pltpu.make_async_remote_copy(
+            grad_send.at[k], grad_recv.at[k], gr_send.at[k], gr_recv.at[k], where, pl.DeviceIdType.MESH
+        )
+
+    def weight_copy(k):
+        where = {"sp": lax.rem(me + k, n)}
+        return pltpu.make_async_remote_copy(
+            w_send.at[k], w_recv.at[k], wt_send.at[k], wt_recv.at[k], where, pl.DeviceIdType.MESH
+        )
+
+    for k in range(1, n):
+        @pl.when(me + k < n)
+        def _(k=k):
+            for copy in kv_copy(k):
+                copy.start()
+    for k in range(1, m):
+        norm_copy(k).start()
+
+    for load in loads[3:]:
+        load.wait()
+    low = lax.broadcasted_iota(jnp.int32, (tokens, 2 * HDIM), 1) < HDIM
+    for pair in range(groups // 2):
+        lanes = pl.ds(2 * HDIM * pair, 2 * HDIM)
+        two = q_in[:, lanes].astype(F32) * scale
+        up = cot_in[:, lanes].astype(F32)
+        for half in range(2):
+            head = 2 * pair + half
+            q_head = two if half == 0 else pltpu.roll(two, HDIM, 1)
+            c_head = up if half == 1 else pltpu.roll(up, HDIM, 1)
+            diag[pl.ds(head * tokens, tokens), :] = jnp.where(low, q_head, 0.0).astype(BF16)
+            diag[pl.ds(span + head * tokens, tokens), :] = jnp.where(low, 0.0, c_head).astype(BF16)
+    product = out_in[...].astype(F32) * cot_in[...].astype(F32)
+    delta = jnp.sum(product.T.reshape(groups, HDIM, tokens), axis=1)
+    row_term = local - lse_in[...]
+
+    def visit(k, key_rows):
+        block = kv[k]
+        both = dot(block, diag[...], NT)
+        key_cols = key_rows.T
+        prob_parts, score_parts = ([], [])
+        for h in range(groups):
+            score = both[:, h * tokens : (h + 1) * tokens] + (row_term[h : h + 1, :] + key_cols[:, h : h + 1])
+            if k == 0:
+                score = jnp.where(rows <= cols, score, NEG_LARGE)
+            prob = jnp.exp(score)
+            dprob = both[:, span + h * tokens : span + (h + 1) * tokens]
+            prob_parts.append(prob.astype(BF16))
+            score_parts.append((prob * (dprob - delta[h : h + 1, :])).astype(BF16))
+        dscore = jnp.concatenate(score_parts, axis=1)
+        weights = jnp.concatenate(score_parts + prob_parts, axis=1)
+        grads = dot(weights, diag[...])
+        key_t = block.T[:HDIM, :]
+        dq_add = dot(key_t, dscore)
+        if k == 0:
+            dq[...] = dq_add
+            grad_own[...] = grads
+        else:
+            dq[...] += dq_add
+            grad_send[k] = grads.astype(BF16)
+
+    visit(0, jnp.concatenate([-local, -local], axis=0))
+
+    for k in range(1, n):
+        @pl.when(k <= me)
+        def _(k=k):
+            for copy in kv_copy(k):
+                copy.wait_recv()
+            key_rows = gates[k, 0:groups, :]
+            for between in range(1, k):
+                key_rows = key_rows + gates[between, groups:, :]
+            visit(k, jnp.concatenate([key_rows, key_rows], axis=0))
+            grad_copy(k).start()
+
+    for pair in range(groups // 2):
+        first = dq[:, pl.ds(2 * pair * tokens, tokens)]
+        second = dq[:, pl.ds((2 * pair + 1) * tokens, tokens)]
+        joined = jnp.concatenate([first, second], axis=0) * scale
+        qg_ref[:, pl.ds(2 * HDIM * pair, 2 * HDIM)] = joined.T.astype(BF16)
+
+    for k in range(1, n):
+        @pl.when(me + k < n)
+        def _(k=k):
+            grad_copy(k).wait_recv()
+            grad_own[...] += grad_recv[k].astype(F32)
+    grads = grad_own[...]
+    kg_ref[...] = grads[:, :HDIM].astype(BF16)
+    vg_ref[...] = grads[:, HDIM:].astype(BF16)
+    key_grad_t = grads.T[:HDIM, :].astype(BF16)
+
+    for k in range(1, m):
+        norm_arrival(k).wait_recv()
+    for k in range(1, n):
+        w_send[k] = dot(key_grad_t, normed_all[lax.rem(me + k, n)]).astype(BF16)
+        weight_copy(k).start()
+    w_own[...] = dot(key_grad_t, normed_all[me])
+    for k in range(1, n):
+        weight_copy(k).wait_recv()
+        w_own[...] += w_recv[k].astype(F32)
+    wg_ref[...] = w_own[...].T
+
+    for k in range(1, m):
+        norm_copy(k).wait_send()
+    for k in range(1, n):
+        weight_copy(k).wait_send()
+
+        @pl.when(me + k < n)
+        def _(k=k):
+            for copy in kv_copy(k):
+                copy.wait_send()
+
+        @pl.when(k <= me)
+        def _(k=k):
+            grad_copy(k).wait_send()
+
+
+def one_kernel(n, m, queries, keys, values, log_gate, log_sum, output, cotangent, normed):
+    tokens, width = queries.shape
+    kv_width = keys.shape[1]
+    groups = log_gate.shape[0]
+    per = n // m
+    chunk = normed.shape[1] // per
+    pair = 2 * HDIM
+    vmem = pltpu.VMEM
+    dma = pltpu.SemaphoreType.DMA
+    full = pl.BlockSpec(memory_space=pltpu.VMEM)
+    return tuple(
+        pl.pallas_call(
+            functools.partial(fused, n, m),
+            out_shape=(
+                jax.ShapeDtypeStruct((tokens, width), BF16),
+                jax.ShapeDtypeStruct((tokens, kv_width), BF16),
+                jax.ShapeDtypeStruct((tokens, kv_width), BF16),
+                jax.ShapeDtypeStruct((chunk, kv_width), F32),
+            ),
+            in_specs=[HBM] * 8,
+            out_specs=(full,) * 4,
+            scratch_shapes=[
+                vmem((tokens, width), BF16), vmem((tokens, kv_width), BF16), vmem((tokens, kv_width), BF16),
+                vmem((groups, tokens), F32), vmem((groups, tokens), F32),
+                vmem((tokens, width), BF16), vmem((tokens, width), BF16),
+                vmem((n, tokens, chunk), BF16), vmem((n, tokens, pair), BF16), vmem((n, 2 * groups, tokens), F32),
+                vmem((2 * groups * tokens, pair), BF16), vmem((HDIM, groups * tokens), F32),
+                vmem((n, tokens, pair), BF16), vmem((n, tokens, pair), BF16), vmem((tokens, pair), F32),
+                vmem((n, HDIM, chunk), BF16), vmem((n, HDIM, chunk), BF16), vmem((HDIM, chunk), F32),
+                dma((7,)), dma((per,)), dma((m,)), dma((m,)), dma((n,)), dma((n,)), dma((n,)), dma((n,)),
+                dma((n,)), dma((n,)), dma((n,)), dma((n,)),
+            ],
+            compiler_params=pltpu.CompilerParams(collective_id=0, has_side_effects=True),
+        )(queries, keys, values, log_gate, log_sum, output, cotangent, normed)
+    )
+
+
+def chosen(n, m, *arrays):
+    queries, keys, log_gate, normed = (arrays[0], arrays[1], arrays[3], arrays[7])
+    whole = (
+        n % m == 0
+        and keys.shape[1] == HDIM
+        and log_gate.shape[0] == 4
+        and queries.shape[0] == 128
+        and normed.shape[1] % (n // m * 128) == 0
+    )
+    return one_kernel(n, m, *arrays) if whole else body(*arrays)
+
+
 def solution(mesh):
+    n_sp, n_tp = mesh.shape["sp"], mesh.shape["tp"]
     in_specs = (
         P("sp", "tp"),
         P("sp", "tp"),
@@ -178,4 +433,4 @@
         P("sp", "tp"),
     )
     out_specs = (P("sp", "tp"), P("sp", "tp"), P("sp", "tp"), P("sp", "tp"))
-    return jax.shard_map(body, mesh=mesh, in_specs=in_specs, out_specs=out_specs, check_vma=False)
+    return jax.shard_map(functools.partial(chosen, n_sp, n_tp), mesh=mesh, in_specs=in_specs, out_specs=out_specs, check_vma=False)

time: 178 us -> 34.3 us (0.19)
  waiting for transfers between devices: 73.4 us -> 0 us
  starting transfers between devices: 41.6 us -> 0 us
  blocking collectives: 30.3 us -> 0 us
  Pallas kernels: 0 us -> 26.8 us
  between operations: 15.8 us -> 0.66 us
  matrix products: 4.19 us -> 0 us
  other arithmetic: 3.18 us -> 0 us
    reduce_scatter x1 -> x0, waiting for transfers between devices: 63.9 us -> none  [body(): lax.psum_scatter(lax.dot_general(whole_rows, key_grad, (((0,), (0,)), (()...]
    ppermute x22 -> x0, starting transfers between devices: 41.5 us -> none  [the longest x21 41.5 us: shifted(): return lax.ppermute(x, axis, pairs)]
    pallas_call x0 -> x1, Pallas kernels: none -> 26.8 us  [one_kernel(): pl.pallas_call(functools.partial(fused, n, m), out_shape=(jax.ShapeDtypeS...]
    unnamed x1 -> x0, blocking collectives: 23.1 us -> none
    ppermute x22 -> x0, waiting for transfers between devices: 9.54 us -> none  [the longest x21 9.53 us: shifted(): return lax.ppermute(x, axis, pairs)]
    all_gather x1 -> x0, blocking collectives: 7.21 us -> none  [body(): whole_rows = lax.all_gather(normed, 'tp', axis=1, tiled=True)]
    dot_general x6 -> x0, matrix products: 4.19 us -> none  [the longest x1 1.48 us: attend(): jnp.einsum('qhgd,khd->hgqk', query_split, key_part, preferred_element_typ...]
    pallas_call x0 -> x3, local copies, waits for them, and re-layouts: none -> 3.8 us  [one_kernel(): pl.pallas_call(functools.partial(fused, n, m), out_shape=(jax.ShapeDtypeS...]
  transfers between devices with their start and end apart: 23 -> 0, of which waited for: 7 -> 0; matrix products, arithmetic and copies ran while one was open for 3% -> 0% of each run, Pallas kernels for 0% -> 0%
where the time goes in v1:
time: 34.3 us; the launch traced here: 34 us
  Pallas kernels  26.8 us (78%)
  local copies, waits for them, and re-layouts  6.6 us (19%)
  between operations  0.66 us (2%)
    pallas_call x1, Pallas kernels, one_kernel(): pl.pallas_call(functools.partial(fused, n, m), out_shape=(jax.ShapeDtypeS...  26.8 us
    pallas_call x3, local copies, waits for them, and re-layouts, one_kernel(): pl.pallas_call(functools.partial(fused, n, m), out_shape=(jax.ShapeDtypeS...  3.8 us
    unnamed x9, local copies, waits for them, and re-layouts  2.8 us

profile of v1, /device:TPU:0, one launch (start us, length us, event | category | flops | bytes accessed | tf_op | source)
XLA Modules:
  0.0 34.0 jit_solution(625626710373741774)
XLA Ops:
  0.6 0.0 copy-start.2
  0.6 1.4 %copy.12.k_hbm = bf16[128,64]{1,0:T(8,128)(2,1)} copy(bf16[128,64]{0,1:T(8,128)(2,1)} %param.9) | data formatting | bytes 32768 | tf_op args[1]
  2.1 0.0 copy-done.2
  2.1 0.7 %copy.13.v_hbm = bf16[128,64]{1,0:T(8,128)(2,1)} copy(bf16[128,64]{0,1:T(8,128)(2,1)S(1)} %copy-done.2) | data formatting | bytes 32768 | tf_op args[2]
  2.8 26.8 %shard_map.111 = (bf16[128,256]{1,0:T(8,128)(2,1)}, bf16[128,64]{1,0:T(8,128)(2,1)}, bf16[128,64]{1,0:T(8,128)(2,1)}, f32[256,64]{1,0:T(8,128)}) custom-call(bf16[128,256]{1,0:T(8,128)(2,1)} %q_hbm.1, bf16[128,64]{1,0:T(8,128)(2,1)} %copy.12.k_hbm, bf16[128,64]{1,0:T(8,128)(2,1)} %copy.13.v_hbm, f32[4,128]{1,0:T(4,128)} %gate_hbm.1, f32[4,128]{1,0:T(4,128)} %lse_hbm.1, ...), custom_call_target="tpu_custom_call" | custom-call | tf_op jit(solution)/shard_map/pallas_call | solution.py:385
  29.6 0.0 copy-start.1
  29.6 1.5 %copy.14 = bf16[128,64]{0,1:T(8,128)(2,1)} copy(bf16[128,64]{1,0:T(8,128)(2,1)} %get-tuple-element.5) | data formatting | bytes 32768 | tf_op jit(solution)/shard_map/pallas_call | solution.py:385
  31.0 0.0 copy-done.1
  31.0 0.7 %copy.15 = bf16[128,64]{0,1:T(8,128)(2,1)} copy(bf16[128,64]{1,0:T(8,128)(2,1)S(1)} %copy-done.1) | data formatting | bytes 32768 | tf_op jit(solution)/shard_map/pallas_call | solution.py:385
  31.7 0.0 copy-start
  31.7 1.6 %copy.16 = f32[256,64]{0,1:T(8,128)} copy(f32[256,64]{1,0:T(8,128)} %get-tuple-element.7) | data formatting | bytes 131072 | tf_op jit(solution)/shard_map/pallas_call | solution.py:385
  33.4 0.0 copy-done
  33.4 0.6 %copy.18 = bf16[128,256]{1,0:T(8,128)(2,1)} copy(bf16[128,256]{1,0:T(8,128)(2,1)S(1)} %copy-done) | data formatting | bytes 131072
Async XLA Ops:
  0.6 1.5 %copy-start.2 = (bf16[128,64]{0,1:T(8,128)(2,1)S(1)}, bf16[128,64]{0,1:T(8,128)(2,1)}, u32[]{:S(2)}) copy-start(bf16[128,64]{0,1:T(8,128)(2,1)} %param.10) | copy-start | bytes 49156
  29.6 1.5 %copy-start.1 = (bf16[128,64]{1,0:T(8,128)(2,1)S(1)}, bf16[128,64]{1,0:T(8,128)(2,1)}, u32[]{:S(2)}) copy-start(bf16[128,64]{1,0:T(8,128)(2,1)} %get-tuple-element.6) | copy-start | bytes 49156
  31.7 1.7 %copy-start = (bf16[128,256]{1,0:T(8,128)(2,1)S(1)}, bf16[128,256]{1,0:T(8,128)(2,1)}, u32[]{:S(2)}) copy-start(bf16[128,256]{1,0:T(8,128)(2,1)} %get-tuple-element.12) | copy-start | bytes 196612

commit v2 on v1

--- a/solution.py
+++ b/solution.py
@@ -184,8 +184,8 @@
     n, m,
     q_hbm, k_hbm, v_hbm, gate_hbm, lse_hbm, out_hbm, cot_hbm, normed_hbm,
     qg_ref, kg_ref, vg_ref, wg_ref,
-    q_in, k_in, v_in, gate_in, lse_in, out_in, cot_in,
-    normed_all, kv, gates, diag, dq, grad_send, grad_recv, grad_own, w_send, w_recv, w_own,
+    q_in, gate_in, lse_in, out_in, cot_in,
+    normed_all, kv, gates, diag, dq, grad_send, grad_recv, grad_own, w_send, w_recv,
     in_sem, norm_in_sem, norm_send, norm_recv, kv_send, kv_recv, gate_send, gate_recv,
     gr_send, gr_recv, wt_send, wt_recv,
 ):
@@ -205,7 +205,7 @@
         pl.semaphore_signal(barrier, inc=1, device_id={"tp": lax.rem(tp + k, m)}, device_id_type=pl.DeviceIdType.MESH)
 
     pairs = [
-        (k_hbm, k_in), (v_hbm, v_in), (gate_hbm, gate_in), (q_hbm, q_in), (cot_hbm, cot_in),
+        (k_hbm, kv.at[0, pl.ds(0, HDIM)]), (v_hbm, kv.at[0, pl.ds(HDIM, HDIM)]), (gate_hbm, gate_in), (q_hbm, q_in), (cot_hbm, cot_in),
         (out_hbm, out_in), (lse_hbm, lse_in),
     ]
     loads = [pltpu.make_async_copy(a, b, in_sem.at[i]) for i, (a, b) in enumerate(pairs)]
@@ -222,7 +222,6 @@
 
     for load in loads[:3]:
         load.wait()
-    kv[0] = jnp.concatenate([k_in[...], v_in[...]], axis=1)
     rows = lax.broadcasted_iota(jnp.int32, (tokens, tokens), 0)
     cols = lax.broadcasted_iota(jnp.int32, (tokens, tokens), 1)
     gate = gate_in[...]
@@ -293,7 +292,7 @@
 
     def visit(k, key_rows):
         block = kv[k]
-        both = dot(block, diag[...], NT)
+        both = dot(block.T, diag[...], NT)
         key_cols = key_rows.T
         prob_parts, score_parts = ([], [])
         for h in range(groups):
@@ -307,8 +306,7 @@
         dscore = jnp.concatenate(score_parts, axis=1)
         weights = jnp.concatenate(score_parts + prob_parts, axis=1)
         grads = dot(weights, diag[...])
-        key_t = block.T[:HDIM, :]
-        dq_add = dot(key_t, dscore)
+        dq_add = dot(block[:HDIM, :], dscore)
         if k == 0:
             dq[...] = dq_add
             grad_own[...] = grads
@@ -340,21 +338,20 @@
         def _(k=k):
             grad_copy(k).wait_recv()
             grad_own[...] += grad_recv[k].astype(F32)
-    grads = grad_own[...]
-    kg_ref[...] = grads[:, :HDIM].astype(BF16)
-    vg_ref[...] = grads[:, HDIM:].astype(BF16)
-    key_grad_t = grads.T[:HDIM, :].astype(BF16)
+    grads = grad_own[...].T.astype(BF16)
+    key_grad_t = grads[:HDIM, :]
+    kg_ref[...] = key_grad_t
+    vg_ref[...] = grads[HDIM:, :]
 
     for k in range(1, m):
         norm_arrival(k).wait_recv()
     for k in range(1, n):
         w_send[k] = dot(key_grad_t, normed_all[lax.rem(me + k, n)]).astype(BF16)
         weight_copy(k).start()
-    w_own[...] = dot(key_grad_t, normed_all[me])
+    wg_ref[...] = dot(key_grad_t, normed_all[me])
     for k in range(1, n):
         weight_copy(k).wait_recv()
-        w_own[...] += w_recv[k].astype(F32)
-    wg_ref[...] = w_own[...].T
+        wg_ref[...] += w_recv[k].astype(F32)
 
     for k in range(1, m):
         norm_copy(k).wait_send()
@@ -381,31 +378,30 @@
     vmem = pltpu.VMEM
     dma = pltpu.SemaphoreType.DMA
     full = pl.BlockSpec(memory_space=pltpu.VMEM)
-    return tuple(
-        pl.pallas_call(
+    query_grad, key_grad, value_grad, weight_grad = pl.pallas_call(
             functools.partial(fused, n, m),
             out_shape=(
                 jax.ShapeDtypeStruct((tokens, width), BF16),
-                jax.ShapeDtypeStruct((tokens, kv_width), BF16),
-                jax.ShapeDtypeStruct((tokens, kv_width), BF16),
-                jax.ShapeDtypeStruct((chunk, kv_width), F32),
+                jax.ShapeDtypeStruct((kv_width, tokens), BF16),
+                jax.ShapeDtypeStruct((kv_width, tokens), BF16),
+                jax.ShapeDtypeStruct((kv_width, chunk), F32),
             ),
             in_specs=[HBM] * 8,
             out_specs=(full,) * 4,
             scratch_shapes=[
-                vmem((tokens, width), BF16), vmem((tokens, kv_width), BF16), vmem((tokens, kv_width), BF16),
+                vmem((tokens, width), BF16),
                 vmem((groups, tokens), F32), vmem((groups, tokens), F32),
                 vmem((tokens, width), BF16), vmem((tokens, width), BF16),
                 vmem((n, tokens, chunk), BF16), vmem((n, tokens, pair), BF16), vmem((n, 2 * groups, tokens), F32),
                 vmem((2 * groups * tokens, pair), BF16), vmem((HDIM, groups * tokens), F32),
                 vmem((n, tokens, pair), BF16), vmem((n, tokens, pair), BF16), vmem((tokens, pair), F32),
-                vmem((n, HDIM, chunk), BF16), vmem((n, HDIM, chunk), BF16), vmem((HDIM, chunk), F32),
+                vmem((n, HDIM, chunk), BF16), vmem((n, HDIM, chunk), BF16),
                 dma((7,)), dma((per,)), dma((m,)), dma((m,)), dma((n,)), dma((n,)), dma((n,)), dma((n,)),
                 dma((n,)), dma((n,)), dma((n,)), dma((n,)),
             ],
             compiler_params=pltpu.CompilerParams(collective_id=0, has_side_effects=True),
-        )(queries, keys, values, log_gate, log_sum, output, cotangent, normed)
-    )
+        )(queries, keys.T, values.T, log_gate, log_sum, output, cotangent, normed)
+    return (query_grad, key_grad.T, value_grad.T, weight_grad.T)
 
 
 def chosen(n, m, *arrays):

time: 34.3 us -> 30.8 us (0.90)
  local copies, waits for them, and re-layouts: 6.6 us -> 3.34 us
    pallas_call x3 -> x0, local copies, waits for them, and re-layouts: 3.8 us -> none  [one_kernel(): pl.pallas_call(functools.partial(fused, n, m), out_shape=(jax.ShapeDtypeS...]
    unnamed x9 -> x10, local copies, waits for them, and re-layouts: 2.8 us -> 3.34 us
where the time goes in v2:
time: 30.8 us; the launch traced here: 30.6 us
  Pallas kernels  26.6 us (86%)
  local copies, waits for them, and re-layouts  3.34 us (11%)
  between operations  0.66 us (2%)
    pallas_call x1, Pallas kernels, one_kernel(): pl.pallas_call(functools.partial(fused, n, m), out_shape=(jax.ShapeDtypeS...  26.6 us
    unnamed x10, local copies, waits for them, and re-layouts  3.34 us

profile of v2, /device:TPU:0, one launch (start us, length us, event | category | flops | bytes accessed | tf_op | source)
XLA Modules:
  0.0 30.6 jit_solution(6325147664774558579)
XLA Ops:
  0.6 26.6 %shard_map.111 = (bf16[128,256]{1,0:T(8,128)(2,1)}, bf16[64,128]{1,0:T(8,128)(2,1)}, bf16[64,128]{1,0:T(8,128)(2,1)}, f32[64,256]{1,0:T(8,128)}) custom-call(bf16[128,256]{1,0:T(8,128)(2,1)} %q_hbm.1, bf16[64,128]{1,0:T(8,128)(2,1)} %bitcast.6, bf16[64,128]{1,0:T(8,128)(2,1)} %bitcast.7, f32[4,128]{1,0:T(4,128)} %gate_hbm.1, f32[4,128]{1,0:T(4,128)} %lse_hbm.1, ...), custom_call_target="tpu_custom_call" | custom-call | tf_op jit(solution)/shard_map/pallas_call | solution.py:381
  27.2 0.0 copy-start.2
  27.2 0.0 copy-start.1
  27.2 1.5 %copy.16 = bf16[128,256]{1,0:T(8,128)(2,1)} copy(bf16[128,256]{1,0:T(8,128)(2,1)} %get-tuple-element.16) | data formatting | bytes 131072
  28.7 0.0 copy-done.2
  28.7 0.0 copy-start
  28.7 0.6 %copy.17 = bf16[128,64]{0,1:T(8,128)(2,1)} copy(bf16[128,64]{0,1:T(8,128)(2,1)S(1)} %bitcast.9) | data formatting | bytes 32768
  29.3 0.0 copy-done.1
  29.3 0.6 %copy.18 = bf16[128,64]{0,1:T(8,128)(2,1)} copy(bf16[128,64]{0,1:T(8,128)(2,1)S(1)} %bitcast.8) | data formatting | bytes 32768
  29.9 0.0 copy-done
  29.9 0.6 %copy.19 = f32[256,64]{0,1:T(8,128)} copy(f32[256,64]{0,1:T(8,128)S(1)} %bitcast.5) | data formatting | bytes 131072
Async XLA Ops:
  27.2 1.5 %copy-start.2 = (bf16[64,128]{1,0:T(8,128)(2,1)S(1)}, bf16[64,128]{1,0:T(8,128)(2,1)}, u32[]{:S(2)}) copy-start(bf16[64,128]{1,0:T(8,128)(2,1)} %get-tuple-element.9) | copy-start | bytes 49156
  27.2 2.1 %copy-start.1 = (bf16[64,128]{1,0:T(8,128)(2,1)S(1)}, bf16[64,128]{1,0:T(8,128)(2,1)}, u32[]{:S(2)}) copy-start(bf16[64,128]{1,0:T(8,128)(2,1)} %get-tuple-element.10) | copy-start | bytes 49156
  28.7 1.2 %copy-start = (f32[64,256]{1,0:T(8,128)S(1)}, f32[64,256]{1,0:T(8,128)}, u32[]{:S(2)}) copy-start(f32[64,256]{1,0:T(8,128)} %get-tuple-element.11) | copy-start | bytes 196612

commit v3 on v2

--- a/solution.py
+++ b/solution.py
@@ -180,13 +180,26 @@
     return lax.dot_general(a, b, dims, precision=precision, preferred_element_type=F32)
 
 
+def split(x):
+    high = x.astype(BF16).astype(F32)
+    middle = (x - high).astype(BF16).astype(F32)
+    parts = [high, middle, x - high - middle, jnp.zeros_like(x)]
+    return jnp.concatenate(parts, axis=0).astype(BF16)
+
+
+def unsplit(parts):
+    wide = parts.astype(F32)
+    rows = wide.shape[0] // 4
+    return wide[:rows] + wide[rows : 2 * rows] + wide[2 * rows : 3 * rows]
+
+
 def fused(
     n, m,
     q_hbm, k_hbm, v_hbm, gate_hbm, lse_hbm, out_hbm, cot_hbm, normed_hbm,
     qg_ref, kg_ref, vg_ref, wg_ref,
     q_in, gate_in, lse_in, out_in, cot_in,
-    normed_all, kv, gates, diag, dq, grad_send, grad_recv, grad_own, w_send, w_recv,
-    in_sem, norm_in_sem, norm_send, norm_recv, kv_send, kv_recv, gate_send, gate_recv,
+    normed_all, kv, sums, diag, dq, grad_send, grad_recv, grad_own, w_send, w_recv,
+    in_sem, norm_in_sem, norm_send, norm_recv, kv_send, kv_recv,
     gr_send, gr_recv, wt_send, wt_recv,
 ):
     me = lax.axis_index("sp")
@@ -227,51 +240,7 @@
     gate = gate_in[...]
     local = dot(gate, (rows <= cols).astype(F32), NN, lax.Precision.HIGHEST)
     total = jnp.broadcast_to(jnp.sum(gate, axis=1, keepdims=True), gate.shape)
-    gates[0, 0:groups, :] = total - local
-    gates[0, groups:, :] = total
-
-    for load in norm_loads:
-        load.wait()
-    pl.semaphore_wait(barrier, n - 1 + m - 1)
-
-    def kv_copy(k):
-        where = {"sp": lax.rem(me + k, n)}
-        return (
-            pltpu.make_async_remote_copy(gates.at[0], gates.at[k], gate_send.at[k], gate_recv.at[k], where, pl.DeviceIdType.MESH),
-            pltpu.make_async_remote_copy(kv.at[0], kv.at[k], kv_send.at[k], kv_recv.at[k], where, pl.DeviceIdType.MESH),
-        )
-
-    def norm_copy(k):
-        mine = normed_all.at[pl.ds(tp * per, per)]
-        return pltpu.make_async_remote_copy(
-            mine, mine, norm_send.at[k], norm_recv.at[k], {"tp": lax.rem(tp + k, m)}, pl.DeviceIdType.MESH
-        )
-
-    def norm_arrival(k):
-        theirs = normed_all.at[pl.ds(lax.rem(tp + m - k, m) * per, per)]
-        return pltpu.make_async_remote_copy(
-            theirs, theirs, norm_send.at[k], norm_recv.at[k], {"tp": lax.rem(tp + k, m)}, pl.DeviceIdType.MESH
-        )
-
-    def grad_copy(k):
-        where = {"sp": lax.rem(me + n - k, n)}
-        return pltpu.make_async_remote_copy(
-            grad_send.at[k], grad_recv.at[k], gr_send.at[k], gr_recv.at[k], where, pl.DeviceIdType.MESH
-        )
-
-    def weight_copy(k):
-        where = {"sp": lax.rem(me + k, n)}
-        return pltpu.make_async_remote_copy(
-            w_send.at[k], w_recv.at[k], wt_send.at[k], wt_recv.at[k], where, pl.DeviceIdType.MESH
-        )
-
-    for k in range(1, n):
-        @pl.when(me + k < n)
-        def _(k=k):
-            for copy in kv_copy(k):
-                copy.start()
-    for k in range(1, m):
-        norm_copy(k).start()
+    kv[0, 2 * HDIM :, :] = split(jnp.concatenate([total - local, total], axis=0))
 
     for load in loads[3:]:
         load.wait()
@@ -290,8 +259,55 @@
     delta = jnp.sum(product.T.reshape(groups, HDIM, tokens), axis=1)
     row_term = local - lse_in[...]
 
+    for load in norm_loads:
+        load.wait()
+    pl.semaphore_wait(barrier, n - 1 + m - 1)
+
+    def kv_copy(k):
+        where = {"sp": lax.rem(me + k, n)}
+        return pltpu.make_async_remote_copy(kv.at[0], kv.at[k], kv_send.at[k], kv_recv.at[k], where, pl.DeviceIdType.MESH)
+
+    def norm_copy(k):
+        mine = normed_all.at[pl.ds(tp * per, per)]
+        return pltpu.make_async_remote_copy(
+            mine, mine, norm_send.at[k], norm_recv.at[k], {"tp": lax.rem(tp + k, m)}, pl.DeviceIdType.MESH
+        )
+
+    def norm_arrival(k):
+        theirs = normed_all.at[pl.ds(lax.rem(tp + m - k, m) * per, per)]
+        return pltpu.make_async_remote_copy(
+            theirs, theirs, norm_send.at[k], norm_recv.at[k], {"tp": lax.rem(tp + k, m)}, pl.DeviceIdType.MESH
+        )
+
+    def grad_copy(k):
+        where = {"sp": lax.rem(me + n - k, n)}
+        return pltpu.make_async_remote_copy(
+            grad_send.at[k], grad_recv.at[k], gr_send.at[k], gr_recv.at[k], where, pl.DeviceIdType.MESH
+        )
+
+    def weight_copy(there):
+        return pltpu.make_async_remote_copy(
+            w_send.at[there], w_recv.at[me], wt_send.at[there], wt_recv.at[me], {"sp": there}, pl.DeviceIdType.MESH
+        )
+
+    def weight_arrival(there):
+        return pltpu.make_async_remote_copy(
+            w_send.at[there], w_recv.at[there], wt_send.at[there], wt_recv.at[there], {"sp": there}, pl.DeviceIdType.MESH
+        )
+
+    def far_first(step):
+        step = step + jnp.where(step >= jnp.where(2 * me < n, n - 1 - me, me), 1, 0)
+        return jnp.where(2 * me < n, n - 1 - step, step)
+
+    for k in range(1, n):
+        @pl.when(me + k < n)
+        def _(k=k):
+            kv_copy(k).start()
+    for k in range(1, m):
+        norm_copy(k).start()
+
     def visit(k, key_rows):
-        block = kv[k]
+        block = kv[k, 0 : 2 * HDIM, :]
         both = dot(block.T, diag[...], NT)
         key_cols = key_rows.T
         prob_parts, score_parts = ([], [])
@@ -319,11 +335,11 @@
     for k in range(1, n):
         @pl.when(k <= me)
         def _(k=k):
-            for copy in kv_copy(k):
-                copy.wait_recv()
-            key_rows = gates[k, 0:groups, :]
+            kv_copy(k).wait_recv()
+            sums[k] = unsplit(kv[k, 2 * HDIM :, :])
+            key_rows = sums[k, 0:groups, :]
             for between in range(1, k):
-                key_rows = key_rows + gates[between, groups:, :]
+                key_rows = key_rows + sums[between, groups:, :]
             visit(k, jnp.concatenate([key_rows, key_rows], axis=0))
             grad_copy(k).start()
 
@@ -345,27 +361,39 @@
 
     for k in range(1, m):
         norm_arrival(k).wait_recv()
-    for k in range(1, n):
-        w_send[k] = dot(key_grad_t, normed_all[lax.rem(me + k, n)]).astype(BF16)
-        weight_copy(k).start()
-    wg_ref[...] = dot(key_grad_t, normed_all[me])
-    for k in range(1, n):
-        weight_copy(k).wait_recv()
-        wg_ref[...] += w_recv[k].astype(F32)
+    for k in range(n - 1):
+        there = far_first(k)
+        w_send[there] = dot(key_grad_t, normed_all[there]).astype(BF16)
+        weight_copy(there).start()
+    weight = dot(key_grad_t, normed_all[me])
+    for k in range(n - 2, -1, -1):
+        there = far_first(k)
+        weight_arrival(there).wait_recv()
+        weight = weight + w_recv[there].astype(F32)
+    wg_ref[...] = weight
 
     for k in range(1, m):
         norm_copy(k).wait_send()
     for k in range(1, n):
-        weight_copy(k).wait_send()
+        weight_copy(far_first(k - 1)).wait_send()
 
         @pl.when(me + k < n)
         def _(k=k):
-            for copy in kv_copy(k):
-                copy.wait_send()
+            kv_copy(k).wait_send()
 
         @pl.when(k <= me)
         def _(k=k):
             grad_copy(k).wait_send()
+
+
+def hand_over(*refs):
+    count = len(refs) // 2
+    sems = refs[-1]
+    copies = [pltpu.make_async_copy(refs[i], refs[count + i], sems.at[i]) for i in range(count)]
+    for copy in copies:
+        copy.start()
+    for copy in copies:
+        copy.wait()
 
 
 def one_kernel(n, m, queries, keys, values, log_gate, log_sum, output, cotangent, normed):
@@ -378,29 +406,35 @@
     vmem = pltpu.VMEM
     dma = pltpu.SemaphoreType.DMA
     full = pl.BlockSpec(memory_space=pltpu.VMEM)
-    query_grad, key_grad, value_grad, weight_grad = pl.pallas_call(
+    shapes = (
+        ((tokens, width), BF16), ((kv_width, tokens), BF16), ((kv_width, tokens), BF16), ((kv_width, chunk), F32)
+    )
+    results = pl.pallas_call(
             functools.partial(fused, n, m),
-            out_shape=(
-                jax.ShapeDtypeStruct((tokens, width), BF16),
-                jax.ShapeDtypeStruct((kv_width, tokens), BF16),
-                jax.ShapeDtypeStruct((kv_width, tokens), BF16),
-                jax.ShapeDtypeStruct((kv_width, chunk), F32),
-            ),
+            out_shape=tuple(vmem(*shape) for shape in shapes),
             in_specs=[HBM] * 8,
             out_specs=(full,) * 4,
             scratch_shapes=[
                 vmem((tokens, width), BF16),
                 vmem((groups, tokens), F32), vmem((groups, tokens), F32),
                 vmem((tokens, width), BF16), vmem((tokens, width), BF16),
-                vmem((n, tokens, chunk), BF16), vmem((n, tokens, pair), BF16), vmem((n, 2 * groups, tokens), F32),
+                vmem((n, tokens, chunk), BF16), vmem((n, pair + 8 * groups, tokens), BF16), vmem((n, 2 * groups, tokens), F32),
                 vmem((2 * groups * tokens, pair), BF16), vmem((HDIM, groups * tokens), F32),
                 vmem((n, tokens, pair), BF16), vmem((n, tokens, pair), BF16), vmem((tokens, pair), F32),
                 vmem((n, HDIM, chunk), BF16), vmem((n, HDIM, chunk), BF16),
-                dma((7,)), dma((per,)), dma((m,)), dma((m,)), dma((n,)), dma((n,)), dma((n,)), dma((n,)),
+                dma((7,)), dma((per,)), dma((m,)), dma((m,)), dma((n,)), dma((n,)),
                 dma((n,)), dma((n,)), dma((n,)), dma((n,)),
             ],
             compiler_params=pltpu.CompilerParams(collective_id=0, has_side_effects=True),
         )(queries, keys.T, values.T, log_gate, log_sum, output, cotangent, normed)
+    results = [pltpu.with_memory_space_constraint(x, pltpu.VMEM) for x in results]
+    query_grad, key_grad, value_grad, weight_grad = pl.pallas_call(
+        hand_over,
+        out_shape=tuple(jax.ShapeDtypeStruct(*shape) for shape in shapes),
+        in_specs=[full] * 4,
+        out_specs=(HBM,) * 4,
+        scratch_shapes=[dma((4,))],
+    )(*results)
     return (query_grad, key_grad.T, value_grad.T, weight_grad.T)
 
 

time: 30.8 us -> 27.8 us (0.903)
  local copies, waits for them, and re-layouts: 3.34 us -> 0 us
    unnamed x10 -> x0, local copies, waits for them, and re-layouts: 3.34 us -> none
    pallas_call x1 -> x2, Pallas kernels: 26.6 us -> 26.9 us  [the longest x1 26.2 us: one_kernel(): pl.pallas_call(functools.partial(fused, n, m), out_shape=tuple((vmem(*sha...]
where the time goes in v3:
time: 27.8 us; the launch traced here: 27.5 us
  Pallas kernels  26.9 us (97%)
  between operations  0.64 us (2%)
    pallas_call x1, Pallas kernels, one_kernel(): pl.pallas_call(functools.partial(fused, n, m), out_shape=tuple((vmem(*sha...  26.2 us
    pallas_call x1, Pallas kernels, one_kernel(): pl.pallas_call(hand_over, out_shape=tuple((jax.ShapeDtypeStruct(*shape) f...  0.7 us

profile of v3, /device:TPU:0, one launch (start us, length us, event | category | flops | bytes accessed | tf_op | source)
XLA Modules:
  0.0 27.5 jit_solution(3672789321127819599)
XLA Ops:
  0.6 26.2 %shard_map.111 = (bf16[128,256]{1,0:T(8,128)(2,1)S(1)}, bf16[64,128]{1,0:T(8,128)(2,1)S(1)}, bf16[64,128]{1,0:T(8,128)(2,1)S(1)}, f32[64,256]{1,0:T(8,128)S(1)}) custom-call(bf16[128,256]{1,0:T(8,128)(2,1)} %q_hbm.1, bf16[64,128]{1,0:T(8,128)(2,1)} %bitcast.5, bf16[64,128]{1,0:T(8,128)(2,1)} %bitcast.6, f32[4,128]{1,0:T(4,128)} %gate_hbm.1, ...), custom_call_target="tpu_custom_call" | custom-call | tf_op jit(solution)/shard_map/pallas_call | solution.py:412
  26.8 0.7 %shard_map.112 = (bf16[128,256]{1,0:T(8,128)(2,1)}, bf16[64,128]{1,0:T(8,128)(2,1)}, bf16[64,128]{1,0:T(8,128)(2,1)}, f32[64,256]{1,0:T(8,128)}) custom-call(bf16[128,256]{1,0:T(8,128)(2,1)S(1)} %get-tuple-element.12.refs_0_, bf16[64,128]{1,0:T(8,128)(2,1)S(1)} %get-tuple-element.13.refs_1_, bf16[64,128]{1,0:T(8,128)(2,1)S(1)} %get-tuple-element.14.refs_2_, ...), custom_call_target="tpu_custom_call" | custom-call | tf_op jit(solution)/shard_map/pallas_call | solution.py:431

commit v4 on v3

--- a/solution.py
+++ b/solution.py
@@ -240,7 +240,7 @@
     gate = gate_in[...]
     local = dot(gate, (rows <= cols).astype(F32), NN, lax.Precision.HIGHEST)
     total = jnp.broadcast_to(jnp.sum(gate, axis=1, keepdims=True), gate.shape)
-    kv[0, 2 * HDIM :, :] = split(jnp.concatenate([total - local, total], axis=0))
+    kv[0, 2 * HDIM :, :] = split(total - local + gate)
 
     for load in loads[3:]:
         load.wait()
@@ -295,9 +295,8 @@
             w_send.at[there], w_recv.at[there], wt_send.at[there], wt_recv.at[there], {"sp": there}, pl.DeviceIdType.MESH
         )
 
-    def far_first(step):
-        step = step + jnp.where(step >= jnp.where(2 * me < n, n - 1 - me, me), 1, 0)
-        return jnp.where(2 * me < n, n - 1 - step, step)
+    def partner(step):
+        return lax.rem(me + n - 1 - step, n)
 
     for k in range(1, n):
         @pl.when(me + k < n)
@@ -305,6 +304,8 @@
             kv_copy(k).start()
     for k in range(1, m):
         norm_copy(k).start()
+
+    last = lax.broadcasted_iota(jnp.int32, (groups, tokens), 1) == tokens - 1
 
     def visit(k, key_rows):
         block = kv[k, 0 : 2 * HDIM, :]
@@ -336,7 +337,10 @@
         @pl.when(k <= me)
         def _(k=k):
             kv_copy(k).wait_recv()
-            sums[k] = unsplit(kv[k, 2 * HDIM :, :])
+            after = unsplit(kv[k, 2 * HDIM :, :])
+            past = pltpu.roll(jnp.concatenate([after, after], axis=0), tokens - 1, 1)[:groups]
+            sums[k, 0:groups, :] = jnp.where(last, 0.0, past)
+            sums[k, groups:, :] = jnp.broadcast_to(after[:, 0:1], after.shape)
             key_rows = sums[k, 0:groups, :]
             for between in range(1, k):
                 key_rows = key_rows + sums[between, groups:, :]
@@ -362,12 +366,12 @@
     for k in range(1, m):
         norm_arrival(k).wait_recv()
     for k in range(n - 1):
-        there = far_first(k)
+        there = partner(k)
         w_send[there] = dot(key_grad_t, normed_all[there]).astype(BF16)
         weight_copy(there).start()
     weight = dot(key_grad_t, normed_all[me])
     for k in range(n - 2, -1, -1):
-        there = far_first(k)
+        there = partner(k)
         weight_arrival(there).wait_recv()
         weight = weight + w_recv[there].astype(F32)
     wg_ref[...] = weight
@@ -375,7 +379,7 @@
     for k in range(1, m):
         norm_copy(k).wait_send()
     for k in range(1, n):
-        weight_copy(far_first(k - 1)).wait_send()
+        weight_copy(partner(k - 1)).wait_send()
 
         @pl.when(me + k < n)
         def _(k=k):
@@ -418,7 +422,7 @@
                 vmem((tokens, width), BF16),
                 vmem((groups, tokens), F32), vmem((groups, tokens), F32),
                 vmem((tokens, width), BF16), vmem((tokens, width), BF16),
-                vmem((n, tokens, chunk), BF16), vmem((n, pair + 8 * groups, tokens), BF16), vmem((n, 2 * groups, tokens), F32),
+                vmem((n, tokens, chunk), BF16), vmem((n, pair + 4 * groups, tokens), BF16), vmem((n, 2 * groups, tokens), F32),
                 vmem((2 * groups * tokens, pair), BF16), vmem((HDIM, groups * tokens), F32),
                 vmem((n, tokens, pair), BF16), vmem((n, tokens, pair), BF16), vmem((tokens, pair), F32),
                 vmem((n, HDIM, chunk), BF16), vmem((n, HDIM, chunk), BF16),

time: 27.8 us -> 26.1 us (0.939)
  Pallas kernels: 26.9 us -> 25.2 us
    pallas_call x1, Pallas kernels: 26.2 us -> 24.5 us  [one_kernel(): pl.pallas_call(functools.partial(fused, n, m), out_shape=tuple((vmem(*sha...]
where the time goes in v4:
time: 26.1 us; the launch traced here: 25.8 us
  Pallas kernels  25.2 us (97%)
  between operations  0.64 us (2%)
    pallas_call x1, Pallas kernels, one_kernel(): pl.pallas_call(functools.partial(fused, n, m), out_shape=tuple((vmem(*sha...  24.5 us
    pallas_call x1, Pallas kernels, one_kernel(): pl.pallas_call(hand_over, out_shape=tuple((jax.ShapeDtypeStruct(*shape) f...  0.7 us

profile of v4, /device:TPU:0, one launch (start us, length us, event | category | flops | bytes accessed | tf_op | source)
XLA Modules:
  0.0 25.8 jit_solution(6297472175094593502)
XLA Ops:
  0.6 24.5 %shard_map.111 = (bf16[128,256]{1,0:T(8,128)(2,1)S(1)}, bf16[64,128]{1,0:T(8,128)(2,1)S(1)}, bf16[64,128]{1,0:T(8,128)(2,1)S(1)}, f32[64,256]{1,0:T(8,128)S(1)}) custom-call(bf16[128,256]{1,0:T(8,128)(2,1)} %q_hbm.1, bf16[64,128]{1,0:T(8,128)(2,1)} %bitcast.5, bf16[64,128]{1,0:T(8,128)(2,1)} %bitcast.6, f32[4,128]{1,0:T(4,128)} %gate_hbm.1, ...), custom_call_target="tpu_custom_call" | custom-call | tf_op jit(solution)/shard_map/pallas_call | solution.py:416
  25.1 0.7 %shard_map.112 = (bf16[128,256]{1,0:T(8,128)(2,1)}, bf16[64,128]{1,0:T(8,128)(2,1)}, bf16[64,128]{1,0:T(8,128)(2,1)}, f32[64,256]{1,0:T(8,128)}) custom-call(bf16[128,256]{1,0:T(8,128)(2,1)S(1)} %get-tuple-element.12.refs_0_, bf16[64,128]{1,0:T(8,128)(2,1)S(1)} %get-tuple-element.13.refs_1_, bf16[64,128]{1,0:T(8,128)(2,1)S(1)} %get-tuple-element.14.refs_2_, ...), custom_call_target="tpu_custom_call" | custom-call | tf_op jit(solution)/shard_map/pallas_call | solution.py:435
